TPU v7x, 128 devices: a whole 4x4x4 slice. The times are simulated.
128 devices in a mesh: kv: 32 (over z, y, core), tp: 4 (over x).
Axes of the slice: x: 4, y: 4, z: 4, core: 2. Of those that a mesh axis runs over, the one named last changes fastest.
Arguments:
- queries: bfloat16 [2, 12288, 1024], P(None, 'kv', 'tp'), may hold values from -112 to 112
- key_states: bfloat16 [2, 12288, 256], P(None, 'kv', 'tp'), may hold values from -4 to 4
- value_states: bfloat16 [2, 12288, 256], P(None, 'kv', 'tp'), may hold values from -6 to 6
- cotangent: bfloat16 [2, 12288, 1024], P(None, 'kv', 'tp'), may hold values from -6 to 6
- gate_logits: float32 [2, 12288, 16], P(None, 'kv', 'tp'), may hold values from -6 to 6
- layer_input: bfloat16 [2, 12288, 4096], P(None, ('kv', 'tp')), may hold values from -6 to 6
- chosen: int32 [2, 192, 4, 16], P(None, 'kv', 'tp'), may hold values from 0 to 191, as said below
Outputs:
- query_grad: bfloat16 [2, 12288, 1024], P(None, 'kv', 'tp')
- key_grad: bfloat16 [2, 12288, 256], P(None, 'kv', 'tp')
- value_grad: bfloat16 [2, 12288, 256], P(None, 'kv', 'tp')
- value_weight_grad: float32 [4096, 256], P(('kv', 'tp'))
Inputs may be any that keep to these rules, and one draw needn't show every extreme that they name: `chosen`: for each sequence, query block b and key head, the 16 entries are distinct blocks; they include b itself and block 0; blocks after b hold only keys after all of the block's queries. Taking the 6 query blocks of one index of kv together (aligned), one sequence and one key head, at most 2 distinct blocks held by any one earlier index of kv are named, and some index reaches 2.
All inputs are finite; a program needn't handle non-finite values.
Results may differ from a plain program's by a relative error of at most 0.0058.
Values may be sent and summed in bfloat16 or wider, within the bound.
A program may use at most 128 MiB of HBM per device.

v0:
```python
import jax
import jax.numpy as jnp
from jax import lax
from jax.experimental import pallas as pl
from jax.experimental.pallas import tpu as pltpu
from jax.sharding import PartitionSpec as P

BLK = 64
MESH = pl.DeviceIdType.MESH
F32 = jnp.float32
BF16 = jnp.bfloat16
SEQS = 2
BPD = 6
ROWS = BPD * BLK
ZN = 4
YN = 4
DEVS = ZN * YN * 2
HD = 64
HEADS = 4
TOPK = 16
NEG = -1e30
HALF = ROWS // 2
QUART = ROWS // 4


def place():
    kv = lax.axis_index("kv")
    tp = lax.axis_index("tp")
    z, y, c = kv // 8, (kv // 2) % 4, kv % 2
    return kv, tp, z, y, c


def rcopy(src, dst, ssem, rsem, device):
    return pltpu.make_async_remote_copy(
        src_ref=src, dst_ref=dst, send_sem=ssem, recv_sem=rsem, device_id=device, device_id_type=MESH
    )


def entry_barrier(peers):
    sem = pltpu.get_barrier_semaphore()
    for peer in peers:
        pl.semaphore_signal(sem, inc=1, device_id=peer, device_id_type=MESH)
    pl.semaphore_wait(sem, len(peers))


class Ring:
    def __init__(self, pos, plus, minus, bufs, ssem, rsem):
        self.pos, self.plus, self.minus = pos, plus, minus
        self.sb, self.rb = bufs
        self.ssem, self.rsem = ssem, rsem
        self.used = []

    def copy(self, i, dev):
        return rcopy(self.sb.at[i], self.rb.at[i], self.ssem.at[i], self.rsem.at[i], dev)

    def send(self, i, dev, value):
        self.sb[i] = value.astype(BF16)
        self.copy(i, dev).start()
        self.used.append((i, dev))

    def got(self, i):
        self.copy(i, self.plus).wait_recv()
        return self.rb[i].astype(F32)

    def start(self, part):
        p = self.pos
        self.send(0, self.plus, part((p + 2) % 4, 0))
        self.send(1, self.minus, part((p + 2) % 4, 1))

    def near(self, part):
        p = self.pos
        self.send(3, self.plus, part((p + 1) % 4, 1))
        self.send(4, self.minus, part((p + 3) % 4, 0))

    def middle(self, part):
        p = self.pos
        self.send(2, self.plus, part((p + 1) % 4, 0) + self.got(0))
        self.send(5, self.minus, part((p + 3) % 4, 1) + self.got(1))

    def end(self, part):
        p = self.pos
        first = part(p, 0) + self.got(2) + self.got(4)
        second = part(p, 1) + self.got(3) + self.got(5)
        return first, second

    def drain(self):
        for i, dev in self.used:
            self.copy(i, dev).wait_send()


class Gather:
    def __init__(self, h, kv_ref, where, ssem, rsem, psend, precv):
        self.h, self.kv_ref, self.where = h, kv_ref, where
        self.ssem, self.rsem, self.psend, self.precv = ssem, rsem, psend, precv
        self.kv, self.tp, self.z, self.y, self.c = where
        self.partner = (self.kv + 1 - 2 * self.c, self.tp)
        self.sends = []
        self.shares = []

    def at(self, a, b):
        dz, dy = (b, a) if self.h == 0 else (a, b)
        return ((self.z + dz) % 4) * 8 + ((self.y + dy) % 4) * 2 + self.c

    def ref(self, a, b, part, shift=0):
        lo, n = self.h * HALF, HALF
        if part is not None:
            lo, n = lo + part * QUART, QUART
        return self.kv_ref.at[self.at(a, b) + shift, pl.ds(lo, n)]

    def copy(self, i, a, b, part, to):
        r = self.ref(a, b, part)
        return rcopy(r, r, self.ssem.at[i], self.rsem.at[i], (self.at(*to), self.tp))

    def send(self, *args):
        self.copy(*args).start()
        self.sends.append(args)

    def recv(self, i, a, b, part):
        self.copy(i, a, b, part, (1, 0)).wait_recv()

    def share_copy(self, n, a, b, shift=0):
        r = self.ref(a, b, None, shift)
        return rcopy(r, r, self.psend.at[n], self.precv.at[n], self.partner)

    def share(self, a, b):
        n = len(self.shares)
        self.shares.append((a, b))
        self.share_copy(n, a, b).start()

    def shared(self):
        for n, (a, b) in enumerate(self.shares):
            self.share_copy(n, a, b, 1 - 2 * self.c).wait_recv()

    def drain(self):
        for args in self.sends:
            self.copy(*args).wait_send()
        for n, (a, b) in enumerate(self.shares):
            self.share_copy(n, a, b).wait_send()

    def first(self):
        self.send(0, 0, 0, None, (1, 0))
        self.send(1, 0, 0, None, (-1, 0))

    def own(self):
        self.second_start(0, 0)
        self.share(0, 0)

    def second_start(self, q, a):
        self.send(4 + 4 * q, a, 0, None, (0, 1))
        self.send(5 + 4 * q, a, 0, None, (0, -1))

    def second_forward(self, q, a):
        self.recv(4 + 4 * q, a, -1, None)
        self.send(6 + 4 * q, a, -1, 0, (0, 1))
        self.recv(5 + 4 * q, a, 1, None)
        self.send(7 + 4 * q, a, 1, 1, (0, -1))
        self.share(a, -1)
        self.share(a, 1)

    def second_end(self, q, a):
        self.recv(6 + 4 * q, a, 2, 0)
        self.recv(7 + 4 * q, a, 2, 1)
        self.share(a, 2)

    def first_forward(self):
        self.recv(0, -1, 0, None)
        self.send(2, -1, 0, 0, (1, 0))
        self.second_start(1, -1)
        self.recv(1, 1, 0, None)
        self.send(3, 1, 0, 1, (-1, 0))
        self.second_start(2, 1)
        self.share(-1, 0)
        self.share(1, 0)

    def first_end(self):
        self.recv(2, 2, 0, 0)
        self.recv(3, 2, 0, 1)
        self.second_start(3, 2)
        self.share(2, 0)


def gather_steps(pair):
    def each(*calls):
        def run():
            for name, *args in calls:
                for g in pair:
                    getattr(g, name)(*args)

        return run

    return [
        each(("first",), ("own",)),
        each(("first_forward",)),
        each(("second_forward", 0, 0), ("first_end",)),
        each(("second_forward", 1, -1), ("second_forward", 2, 1), ("second_end", 0, 0)),
        each(("second_forward", 3, 2), ("second_end", 1, -1), ("second_end", 2, 1)),
        each(("second_end", 3, 2), ("shared",)),
    ]


class Reduce:
    def __init__(self, table, mate, acc, abufs, bbufs, where, s_mate, r_mate, s_ring, r_ring):
        self.table, self.mate, self.acc = table, mate, acc
        self.kv, self.tp, self.z, self.y, self.c = where
        self.s_mate, self.r_mate = s_mate, r_mate
        kv, tp, z, y, c = where
        self.partner = (kv + 1 - 2 * c, tp)

        def to(dz, dy):
            return (((z + dz) % 4) * 8 + ((y + dy) % 4) * 2 + c, tp)

        ydir = (y, to(0, 1), to(0, 3))
        zdir = (z, to(1, 0), to(3, 0))
        self.ra = [
            Ring(*(ydir if h == 0 else zdir), [b.at[h] for b in abufs], s_ring.at[h], r_ring.at[h])
            for h in range(2)
        ]
        self.rb = [
            Ring(*(zdir if h == 0 else ydir), [b.at[h] for b in bbufs], s_ring.at[2 + h], r_ring.at[2 + h])
            for h in range(2)
        ]

    def mate_copy(self, h, g):
        rows = pl.ds(h * HALF, HALF)
        if h == 0:
            src = self.table.at[:, (self.y + g) % 4, 1 - self.c, rows]
            dst = self.mate.at[:, (self.y + g) % 4, rows]
        else:
            src = self.table.at[(self.z + g) % 4, :, 1 - self.c, rows]
            dst = self.mate.at[(self.z + g) % 4, :, rows]
        return rcopy(src, dst, self.s_mate.at[h * 4 + g], self.r_mate.at[h * 4 + g], self.partner)

    def share(self):
        for g in (2, 1, 3, 0):
            for h in range(2):
                self.mate_copy(h, g).start()

    def part_a(self, h):
        rows = slice(h * HALF, (h + 1) * HALF)

        def part(d, q):
            if h == 0:
                a = self.table[2 * q : 2 * q + 2, d, self.c, rows]
                b = self.mate[2 * q : 2 * q + 2, d, rows]
            else:
                a = self.table[d, 2 * q : 2 * q + 2, self.c, rows]
                b = self.mate[d, 2 * q : 2 * q + 2, rows]
            return a.astype(F32) + b.astype(F32)

        return part

    def part_b(self, h):
        def part(d, q):
            return self.acc[h, d, q * QUART : (q + 1) * QUART]

        return part

    def begin(self):
        for h in range(2):
            self.mate_copy(h, 2).wait_recv()
            self.ra[h].start(self.part_a(h))
        for h in range(2):
            self.mate_copy(h, 1).wait_recv()
            self.mate_copy(h, 3).wait_recv()
            self.ra[h].near(self.part_a(h))

    def middle(self):
        for h in range(2):
            self.ra[h].middle(self.part_a(h))

    def turn(self):
        for h in range(2):
            self.mate_copy(h, 0).wait_recv()
            first, second = self.ra[h].end(self.part_a(h))
            self.acc[h, 0:2] = first
            self.acc[h, 2:4] = second
            self.rb[h].start(self.part_b(h))
            self.rb[h].near(self.part_b(h))

    def middle_b(self):
        for h in range(2):
            self.rb[h].middle(self.part_b(h))

    def finish(self, out):
        for h in range(2):
            for q, value in enumerate(self.rb[h].end(self.part_b(h))):
                lo = h * HALF + q * QUART
                out[lo : lo + QUART] = value

    def drain(self):
        for h in range(2):
            for g in range(4):
                self.mate_copy(h, g).wait_send()
            self.ra[h].drain()
            self.rb[h].drain()


def whole_kernel(
    ids_ref, inv_ref, k_ref, v_ref, gate_ref, q_hbm, g_hbm, x_hbm,
    dq_ref, kg_ref, vg_ref, wg_ref,
    kv0, kv1, table0, table1, mate0, mate1, acc0, acc1, sa0, ra0, sa1, ra1, sb0, rb0, sb1, rb1,
    q_in, g_in, x_in, gates_t, rows_all, kvbuf, scores, packed, picks, final,
    li_t, li_in, vsend, vland, rhs, w_out, w_own, w_mate, wsend, wland,
    l_sem, ag_s, ag_r, agp_s, agp_r, s_mate, r_mate, s_ring, r_ring, s_li, r_li, s_x, r_x, s_w, r_w, s_d, r_d,
):
    where = place()
    kv, tp, z, y, c = where
    other = 1 - c
    nrow = HEADS * BLK

    def zy(z_, y_):
        return ((z_ % 4) * 8 + (y_ % 4) * 2 + c, tp)

    partner = (kv + 1 - 2 * c, tp)
    xs = [(kv, (tp + d) % 4) for d in (1, 2, 3)]
    offsets = [(dz, dy) for dz in (2, 1, 3, 0) for dy in (2, 1, 3, 0)][:-1]
    kvs, tables = (kv0, kv1), (table0, table1)

    local = [
        pltpu.make_async_copy(x_hbm, x_in, l_sem.at[0]),
        pltpu.make_async_copy(q_hbm, q_in, l_sem.at[1]),
        pltpu.make_async_copy(g_hbm, g_in, l_sem.at[2]),
    ]
    for d in local:
        d.start()
    for s in range(SEQS):
        kvs[s][kv] = jnp.concatenate([k_ref[s], v_ref[s]], axis=0).T
    entry_barrier([partner] + xs + [zy(z + dz, y + dy) for dz, dy in offsets])

    gathers = [
        [Gather(h, kvs[s], where, ag_s.at[s, h], ag_r.at[s, h], agp_s.at[s, h], agp_r.at[s, h]) for h in range(2)]
        for s in range(SEQS)
    ]
    steps = [gather_steps(pair) for pair in gathers]
    reduces = [
        Reduce(
            tables[s], (mate0, mate1)[s], (acc0, acc1)[s],
            ((sa0, ra0), (sa1, ra1))[s], ((sb0, rb0), (sb1, rb1))[s],
            where, s_mate.at[s], r_mate.at[s], s_ring.at[s], r_ring.at[s],
        )
        for s in range(SEQS)
    ]

    def turn_input(i, carry):
        lo = pl.multiple_of(i * 512, 512)
        for s in range(SEQS):
            t = x_in[s, :, pl.ds(lo, 512)].T.reshape(2, 2, 4, 32, 96)
            for n in range(4):
                li_t[n, pl.ds(i * 2, 2), :, :, s * 96 : (s + 1) * 96] = t[:, :, n]
        return carry

    def li_copy(n):
        to = (tp + n + 1) % 4
        return rcopy(li_t.at[to], li_in.at[tp], s_li.at[n], r_li.at[n], (kv, to))

    def prepare(s, qb):
        lane = lax.broadcasted_iota(jnp.int32, (BLK, 2 * HD), 1)
        low = lane < HD
        rows = pl.ds(pl.multiple_of(qb * BLK, BLK), BLK)
        gates = gates_t[s, rows]
        at = s * BPD + qb
        for h in range(HEADS):
            pair = slice((h // 2) * 128, (h // 2) * 128 + 128)
            qv = q_in[s, rows, pair].astype(F32) * 0.125
            gv = gates[:, h : h + 1] * g_in[s, rows, pair].astype(F32)
            if h % 2 == 0:
                gv = pltpu.roll(gv, HD, 1)
            else:
                qv = pltpu.roll(qv, HD, 1)
            rows_all[at, h * BLK : (h + 1) * BLK] = jnp.where(low, qv, 0.0).astype(BF16)
            rows_all[at, nrow + h * BLK : nrow + (h + 1) * BLK] = jnp.where(low, 0.0, gv).astype(BF16)

    def attend(s, qb):
        at = s * BPD + qb
        kv_ref = kvs[s]
        block = kv * BPD + qb
        picked = [ids_ref[s, qb, 0, k] for k in range(TOPK)]
        for k in range(TOPK):
            kvbuf[k * BLK : (k + 1) * BLK] = kv_ref[picked[k] // BPD, pl.ds((picked[k] % BPD) * BLK, BLK)]
        scores[...] = lax.dot_general(
            kvbuf[...], rows_all[at], (((1,), (1,)), ((), ())), preferred_element_type=F32
        )
        qpos = block * BLK + lax.broadcasted_iota(jnp.int32, (BLK, nrow), 1) % BLK
        ahead = lax.broadcasted_iota(jnp.int32, (BLK, nrow), 0) - qpos

        def masked(k):
            sc = scores[k * BLK : (k + 1) * BLK, :nrow]
            return jnp.where(ahead <= -(picked[k] * BLK), sc, NEG)

        top = None
        for k in range(TOPK):
            m = jnp.max(masked(k).reshape(8, 8, nrow), axis=0)
            top = m if top is None else jnp.maximum(top, m)
        top = jnp.max(top, axis=0, keepdims=True)
        total = jnp.zeros((8, nrow), F32)
        for k in range(TOPK):
            e = jnp.exp(masked(k) - top)
            scores[k * BLK : (k + 1) * BLK, :nrow] = e
            total = total + jnp.sum(e.reshape(8, 8, nrow), axis=0)
        scale = 1.0 / jnp.sum(total, axis=0, keepdims=True)
        dot = jnp.zeros((8, nrow), F32)
        for k in range(TOPK):
            rows = slice(k * BLK, (k + 1) * BLK)
            w = (scores[rows, :nrow] * scale).astype(BF16)
            packed[rows, nrow:] = w
            t = w.astype(F32) * scores[rows, nrow:]
            dot = dot + jnp.sum(t.reshape(8, 8, nrow), axis=0)
        row_dot = jnp.sum(dot, axis=0, keepdims=True)
        for k in range(TOPK):
            rows = slice(k * BLK, (k + 1) * BLK)
            ds = (scores[rows, :nrow] * scale) * (scores[rows, nrow:] - row_dot)
            packed[rows, :nrow] = ds.astype(BF16)
        pick = jnp.dot(packed[...], rows_all[at], preferred_element_type=F32)
        picks[pl.ds(qb * TOPK, TOPK)] = pick.reshape(TOPK, BLK, 2 * HD)
        dq_t = jnp.dot(kvbuf[...].T, packed[:, :nrow], preferred_element_type=F32)
        dq = (dq_t[:HD] * 0.125).T
        dq_ref[s, pl.ds(pl.multiple_of(qb * BLK, BLK), BLK)] = jnp.concatenate(
            [dq[h * BLK : (h + 1) * BLK] for h in range(HEADS)], axis=1
        ).astype(BF16)

    def collect(s):
        def one(j, carry):
            for b in range(BPD):
                total = picks[inv_ref[s, 0, j * BPD + b]]
                for q in range(1, BPD):
                    total = total + picks[inv_ref[s, q, j * BPD + b]]
                tables[s][j // 8, (j // 2) % 4, j % 2, b * BLK : (b + 1) * BLK] = total.astype(BF16)
            return carry

        lax.fori_loop(0, DEVS, one, 0)

    quarter = ROWS // 4

    def x_copy(s, n):
        to = (tp + n + 1) % 4
        return rcopy(vsend.at[s], vland.at[s, tp], s_x.at[s, n], r_x.at[s, n], (kv, to))

    def finish(s):
        reduces[s].finish(final)
        lane = lax.broadcasted_iota(jnp.int32, (HALF, 2 * HD), 1)
        low = pltpu.roll(final[0:HALF].astype(BF16).astype(F32), HD, 1)
        value = jnp.where(lane < HD, low, final[HALF:]).astype(BF16)
        vsend[s] = value
        vland[s, tp] = value
        for n in (1, 0, 2):
            x_copy(s, n).start()
        turned = final[...].T
        kg_ref[s] = turned[:HD].astype(BF16)
        vg_ref[s] = turned[HD:].astype(BF16)

    def landed(s):
        for n in range(3):
            frm = (tp + 3 - n) % 4
            slot = vland.at[s, frm]
            rcopy(slot, slot, s_x.at[s, n], r_x.at[s, n], (kv, frm)).wait_recv()
        lane = lax.broadcasted_iota(jnp.int32, (quarter, 2 * HD), 1)
        for t in range(4):
            rows = slice((t % 2) * quarter, (t % 2 + 1) * quarter)
            for p in range(2):
                even = vland[s, 2 * p, rows].astype(F32)
                odd = vland[s, 2 * p + 1, rows].astype(F32)
                if t < 2:
                    odd = pltpu.roll(odd, HD, 1)
                else:
                    even = pltpu.roll(even, HD, 1)
                rhs[t, s * quarter : (s + 1) * quarter, p * 128 : (p + 1) * 128] = jnp.where(
                    lane < HD, even, odd
                ).astype(BF16)

    steps[0][0]()
    local[0].wait()
    lax.fori_loop(0, 8, turn_input, 0)
    for n in (1, 0, 2):
        li_copy(n).start()
    steps[0][1]()
    local[1].wait()
    local[2].wait()
    for s in range(SEQS):
        gates_t[s] = jax.nn.sigmoid(gate_ref[s]).T
    picks[BPD * TOPK] = jnp.zeros((BLK, 2 * HD), F32)
    for n in range(2, 5):
        steps[0][n]()

        def some(i, carry, n=n):
            at = (n - 2) * 4 + i
            prepare(at // BPD, at % BPD)
            return carry

        lax.fori_loop(0, 4, some, 0)
    steps[0][5]()

    def between(n, step):
        def at(qb):
            @pl.when(qb == n)
            def _():
                step()

        return at

    steps[1][0]()
    marks = [between(n, steps[1][n + 1]) for n in range(5)]

    def attend0(qb, carry):
        attend(0, qb)
        for mark in marks:
            mark(qb)
        return carry

    lax.fori_loop(0, BPD, attend0, 0)
    collect(0)
    reduces[0].share()

    late = [reduces[0].begin, reduces[0].middle, reduces[0].turn, reduces[0].middle_b, lambda: finish(0)]
    marks1 = [between(n, late[n]) for n in range(5)]

    def attend1(qb, carry):
        attend(1, qb)
        for mark in marks1:
            mark(qb)
        return carry

    lax.fori_loop(0, BPD, attend1, 0)
    collect(1)
    reduces[1].share()
    landed(0)
    reduces[1].begin()
    reduces[1].middle()
    reduces[1].turn()
    reduces[1].middle_b()
    finish(1)
    for n in range(3):
        frm = (tp + 3 - n) % 4
        rcopy(li_in.at[frm], li_in.at[frm], s_li.at[n], r_li.at[n], (kv, frm)).wait_recv()
    mine_li = pltpu.make_async_copy(li_t.at[tp], li_in.at[tp], l_sem.at[3])
    mine_li.start()
    mine_li.wait()
    landed(1)

    def product(side, i):
        total = None
        for t in range(4):
            a = li_in[t, pl.ds(i * 4, 4), side].reshape(128, 192)
            p = jnp.dot(a, rhs[t], preferred_element_type=F32)
            total = p if total is None else total + p
        return total.reshape(4, 32, 256)

    def for_mate(i, carry):
        w_out[pl.ds(i * 4, 4)] = product(other, i).astype(BF16)
        return carry

    def for_self(i, carry):
        w_own[pl.ds(i * 4, 4)] = product(c, i)
        return carry

    lax.fori_loop(0, 4, for_mate, 0)
    w_copy = rcopy(w_out, w_mate, s_w.at[0], r_w.at[0], partner)
    w_copy.start()
    lax.fori_loop(0, 4, for_self, 0)
    w_copy.wait_recv()
    w_own[...] = w_own[...] + w_mate[...].astype(F32)
    wsend[...] = w_own[...].astype(BF16)
    mine = kv // 2

    def d_copy(n):
        dz, dy = offsets[n]
        to = zy(z + dz, y + dy)
        return rcopy(wsend.at[to[0] // 2], wland.at[mine], s_d.at[n], r_d.at[n], to)

    for n in range(len(offsets)):
        d_copy(n).start()
    total = w_own[mine]
    for n, (dz, dy) in enumerate(offsets):
        frm = zy(z - dz, y - dy)
        slot = wland.at[frm[0] // 2]
        rcopy(slot, slot, s_d.at[n], r_d.at[n], frm).wait_recv()
        total = total + wland[frm[0] // 2].astype(F32)
    wg_ref[...] = total

    for pair in gathers:
        for g in pair:
            g.drain()
    for r in reduces:
        r.drain()
    for n in range(3):
        li_copy(n).wait_send()
        for s in range(SEQS):
            x_copy(s, n).wait_send()
    w_copy.wait_send()
    for n in range(len(offsets)):
        d_copy(n).wait_send()


def whole(chosen, inverse, keys, values, gates, queries, cotangent, layer_input):
    v = pltpu.VMEM
    dma = pltpu.SemaphoreType.DMA
    wide = 2 * HD
    anywhere = pl.BlockSpec(memory_space=pl.ANY)
    onchip = pl.BlockSpec(memory_space=v)
    smem = pl.BlockSpec(memory_space=pltpu.SMEM)
    keys_n = TOPK * BLK
    nrow = HEADS * BLK
    return pl.pallas_call(
        whole_kernel,
        out_shape=[
            jax.ShapeDtypeStruct((SEQS, ROWS, HEADS * HD), BF16),
            jax.ShapeDtypeStruct((SEQS, HD, ROWS), BF16),
            jax.ShapeDtypeStruct((SEQS, HD, ROWS), BF16),
            jax.ShapeDtypeStruct((32, 256), F32),
        ],
        in_specs=[smem, smem, onchip, onchip, onchip, anywhere, anywhere, anywhere],
        out_specs=[onchip] * 4,
        scratch_shapes=[
            *[v((DEVS, ROWS, wide), BF16) for _ in range(2)],
            *[v((ZN, YN, 2, ROWS, wide), BF16) for _ in range(2)],
            *[v((ZN, YN, ROWS, wide), BF16) for _ in range(2)],
            *[v((2, 4, HALF, wide), F32) for _ in range(2)],
            *[v((2, 6, 2, HALF, wide), BF16) for _ in range(4)],
            *[v((2, 6, QUART, wide), BF16) for _ in range(4)],
            v((SEQS, ROWS, HEADS * HD), BF16),
            v((SEQS, ROWS, HEADS * HD), BF16),
            v((SEQS, ROWS // 4, 4096), BF16),
            v((SEQS, ROWS, HEADS), F32),
            v((SEQS * BPD, 2 * nrow, wide), BF16),
            v((keys_n, wide), BF16),
            v((keys_n, 2 * nrow), F32),
            v((keys_n, 2 * nrow), BF16),
            v((BPD * TOPK + 1, BLK, wide), F32),
            v((ROWS, wide), F32),
            v((4, 16, 2, 32, 192), BF16),
            v((4, 16, 2, 32, 192), BF16),
            v((SEQS, HALF, wide), BF16),
            v((SEQS, 4, HALF, wide), BF16),
            v((4, 192, 256), BF16),
            v((16, 32, 256), BF16),
            v((16, 32, 256), F32),
            v((16, 32, 256), BF16),
            v((16, 32, 256), BF16),
            v((16, 32, 256), BF16),
            dma((4,)),
            *[dma((2, 2, 20)) for _ in range(2)],
            *[dma((2, 2, 16)) for _ in range(2)],
            *[dma((2, 8)) for _ in range(2)],
            *[dma((2, 4, 6)) for _ in range(2)],
            *[dma((3,)) for _ in range(2)],
            *[dma((2, 3)) for _ in range(2)],
            *[dma((1,)) for _ in range(2)],
            *[dma((15,)) for _ in range(2)],
        ],
        compiler_params=pltpu.CompilerParams(
            collective_id=0, has_side_effects=True, vmem_limit_bytes=58 * 2**20
        ),
        name="whole",
    )(chosen, inverse, keys, values, gates, queries, cotangent, layer_input)


def on_device(queries, key_states, value_states, cotangent, gate_logits, layer_input, chosen):
    def turned(a):
        return jnp.swapaxes(a, 1, 2)

    blocks = jnp.arange(DEVS * BPD, dtype=jnp.int32)
    order = jnp.arange(TOPK, dtype=jnp.int32)[:, None]
    first = jnp.arange(BPD, dtype=jnp.int32)[:, None, None] * TOPK
    hit = chosen[:, :, 0, :, None] == blocks
    inverse = jnp.min(jnp.where(hit, order + first, BPD * TOPK), axis=2)
    query_grad, key_grad, value_grad, weight_grad = whole(
        chosen, inverse, turned(key_states), turned(value_states), turned(gate_logits),
        queries, cotangent, layer_input,
    )
    return query_grad, turned(key_grad), turned(value_grad), weight_grad


def solution(mesh):
    placed = (
        P(None, "kv", "tp"),
        P(None, "kv", "tp"),
        P(None, "kv", "tp"),
        P(None, "kv", "tp"),
        P(None, "kv", "tp"),
        P(None, ("kv", "tp"), None),
        P(None, "kv", "tp", None),
    )
    return jax.shard_map(
        on_device,
        mesh=mesh,
        in_specs=placed,
        out_specs=(P(None, "kv", "tp"), P(None, "kv", "tp"), P(None, "kv", "tp"), P(("kv", "tp"), None)),
        check_vma=False,
    )
```

profile of v0, /device:TPU:0, one launch (start us, length us, event | category | flops | bytes accessed | tf_op | source)
XLA Modules:
  0.0 111.2 jit_solution(2075826904840036940)
XLA Ops:
  0.6 0.1 iota_add_fusion
  0.7 0.7 copy.16
  1.4 0.8 select_reduce_fusion.inv_ref
  2.2 102.8 %whole.1 = (bf16[2,384,256]{2,1,0:T(8,128)(2,1)}, bf16[2,64,384]{2,1,0:T(8,128)(2,1)}, bf16[2,64,384]{2,1,0:T(8,128)(2,1)}, f32[32,256]{1,0:T(8,128)}) custom-call(s32[2,6,1,16]{3,2,1,0:T(1,128)} %ids_ref.1, s32[2,6,192]{2,1,0:T(8,128)} %select_reduce_fusion.inv_ref, bf16[2,64,384]{2,1,0:T(8,128)(2,1)} %bitcast.8, bf16[2,64,384]{2,1,0:T(8,128)(2,1)} %bitcast.9, ...), custom_call_target="tpu_custom_call" | custom-call | tf_op jit(solution)/shard_map/whole/pallas_call | solution.py:602
  105.0 1.8 %copy.21 = bf16[2,384,256]{2,1,0:T(8,128)(2,1)} copy(bf16[2,384,256]{2,1,0:T(8,128)(2,1)} %get-tuple-element.16) | data formatting | bytes 786432
  106.7 1.5 %copy.22 = bf16[2,384,64]{1,2,0:T(8,128)(2,1)} copy(bf16[2,384,64]{1,2,0:T(8,128)(2,1)} %bitcast.11) | data formatting | bytes 196608
  108.3 1.5 %copy.23 = bf16[2,384,64]{1,2,0:T(8,128)(2,1)} copy(bf16[2,384,64]{1,2,0:T(8,128)(2,1)} %bitcast.10) | data formatting | bytes 196608
  109.8 1.4 %copy.24 = f32[32,256]{1,0:T(8,128)} copy(f32[32,256]{1,0:T(8,128)} %get-tuple-element.19) | data formatting | bytes 65536
  (2 shorter events, 0.0 us)
where the time goes:
time: 112 us; the launch traced here: 111 us
  Pallas kernels  103 us (92%)
  local copies, waits for them, and re-layouts  6.93 us (6%)
    pallas_call x1, Pallas kernels, whole(): pl.pallas_call(whole_kernel, out_shape=[jax.ShapeDtypeStruct((SEQS, ROWS,...  103 us
    unnamed x5, local copies, waits for them, and re-layouts  6.92 us

commit v1 on v0

--- a/solution.py
+++ b/solution.py
@@ -296,10 +296,10 @@
 
 
 def whole_kernel(
-    ids_ref, inv_ref, k_ref, v_ref, gate_ref, q_hbm, g_hbm, x_hbm,
+    ids_ref, inv_ref, k_hbm, v_hbm, gate_hbm, q_hbm, g_hbm, x_hbm,
     dq_ref, kg_ref, vg_ref, wg_ref,
     kv0, kv1, table0, table1, mate0, mate1, acc0, acc1, sa0, ra0, sa1, ra1, sb0, rb0, sb1, rb1,
-    q_in, g_in, x_in, gates_t, rows_all, kvbuf, scores, packed, picks, final,
+    k_ref, v_ref, gate_ref, q_in, g_in, x_in, gates_t, rows_all, kvbuf, scores, packed, picks, final,
     li_t, li_in, vsend, vland, rhs, w_out, w_own, w_mate, wsend, wland,
     l_sem, ag_s, ag_r, agp_s, agp_r, s_mate, r_mate, s_ring, r_ring, s_li, r_li, s_x, r_x, s_w, r_w, s_d, r_d,
 ):
@@ -316,16 +316,19 @@
     offsets = [(dz, dy) for dz in (2, 1, 3, 0) for dy in (2, 1, 3, 0)][:-1]
     kvs, tables = (kv0, kv1), (table0, table1)
 
-    local = [
-        pltpu.make_async_copy(x_hbm, x_in, l_sem.at[0]),
-        pltpu.make_async_copy(q_hbm, q_in, l_sem.at[1]),
-        pltpu.make_async_copy(g_hbm, g_in, l_sem.at[2]),
-    ]
+    pairs = ((k_hbm, k_ref), (v_hbm, v_ref), (x_hbm, x_in), (q_hbm, q_in), (g_hbm, g_in), (gate_hbm, gate_ref))
+    local = [pltpu.make_async_copy(a, b, l_sem.at[n]) for n, (a, b) in enumerate(pairs)]
     for d in local:
         d.start()
+    peers = [partner] + xs + [zy(z + dz, y + dy) for dz, dy in offsets]
+    barrier = pltpu.get_barrier_semaphore()
+    for peer in peers:
+        pl.semaphore_signal(barrier, inc=1, device_id=peer, device_id_type=MESH)
+    local[0].wait()
+    local[1].wait()
     for s in range(SEQS):
         kvs[s][kv] = jnp.concatenate([k_ref[s], v_ref[s]], axis=0).T
-    entry_barrier([partner] + xs + [zy(z + dz, y + dy) for dz, dy in offsets])
+    pl.semaphore_wait(barrier, len(peers))
 
     gathers = [
         [Gather(h, kvs[s], where, ag_s.at[s, h], ag_r.at[s, h], agp_s.at[s, h], agp_r.at[s, h]) for h in range(2)]
@@ -468,18 +471,23 @@
                 ).astype(BF16)
 
     steps[0][0]()
-    local[0].wait()
-    lax.fori_loop(0, 8, turn_input, 0)
+    steps[1][0]()
+    local[2].wait()
+    lax.fori_loop(0, 4, turn_input, 0)
+    steps[0][1]()
+    steps[1][1]()
+    lax.fori_loop(4, 8, turn_input, 0)
     for n in (1, 0, 2):
         li_copy(n).start()
-    steps[0][1]()
-    local[1].wait()
-    local[2].wait()
+    for n in (3, 4, 5):
+        local[n].wait()
     for s in range(SEQS):
         gates_t[s] = jax.nn.sigmoid(gate_ref[s]).T
     picks[BPD * TOPK] = jnp.zeros((BLK, 2 * HD), F32)
     for n in range(2, 5):
         steps[0][n]()
+        if n < 4:
+            steps[1][n]()
 
         def some(i, carry, n=n):
             at = (n - 2) * 4 + i
@@ -497,8 +505,7 @@
 
         return at
 
-    steps[1][0]()
-    marks = [between(n, steps[1][n + 1]) for n in range(5)]
+    marks = [between(0, steps[1][4]), between(2, steps[1][5])]
 
     def attend0(qb, carry):
         attend(0, qb)
@@ -510,8 +517,7 @@
     collect(0)
     reduces[0].share()
 
-    late = [reduces[0].begin, reduces[0].middle, reduces[0].turn, reduces[0].middle_b, lambda: finish(0)]
-    marks1 = [between(n, late[n]) for n in range(5)]
+    marks1 = [between(1, reduces[0].begin), between(3, reduces[0].middle), between(5, reduces[0].turn)]
 
     def attend1(qb, carry):
         attend(1, qb)
@@ -522,16 +528,18 @@
     lax.fori_loop(0, BPD, attend1, 0)
     collect(1)
     reduces[1].share()
-    landed(0)
+    reduces[0].middle_b()
     reduces[1].begin()
     reduces[1].middle()
+    finish(0)
     reduces[1].turn()
+    landed(0)
     reduces[1].middle_b()
     finish(1)
     for n in range(3):
         frm = (tp + 3 - n) % 4
         rcopy(li_in.at[frm], li_in.at[frm], s_li.at[n], r_li.at[n], (kv, frm)).wait_recv()
-    mine_li = pltpu.make_async_copy(li_t.at[tp], li_in.at[tp], l_sem.at[3])
+    mine_li = pltpu.make_async_copy(li_t.at[tp], li_in.at[tp], l_sem.at[6])
     mine_li.start()
     mine_li.wait()
     landed(1)
@@ -594,7 +602,7 @@
     v = pltpu.VMEM
     dma = pltpu.SemaphoreType.DMA
     wide = 2 * HD
-    anywhere = pl.BlockSpec(memory_space=pl.ANY)
+    anywhere = pl.BlockSpec(memory_space=pltpu.HBM)
     onchip = pl.BlockSpec(memory_space=v)
     smem = pl.BlockSpec(memory_space=pltpu.SMEM)
     keys_n = TOPK * BLK
@@ -607,7 +615,7 @@
             jax.ShapeDtypeStruct((SEQS, HD, ROWS), BF16),
             jax.ShapeDtypeStruct((32, 256), F32),
         ],
-        in_specs=[smem, smem, onchip, onchip, onchip, anywhere, anywhere, anywhere],
+        in_specs=[smem, smem] + [anywhere] * 6,
         out_specs=[onchip] * 4,
         scratch_shapes=[
             *[v((DEVS, ROWS, wide), BF16) for _ in range(2)],
@@ -616,6 +624,9 @@
             *[v((2, 4, HALF, wide), F32) for _ in range(2)],
             *[v((2, 6, 2, HALF, wide), BF16) for _ in range(4)],
             *[v((2, 6, QUART, wide), BF16) for _ in range(4)],
+            v((SEQS, HD, ROWS), BF16),
+            v((SEQS, HD, ROWS), BF16),
+            v((SEQS, HEADS, ROWS), F32),
             v((SEQS, ROWS, HEADS * HD), BF16),
             v((SEQS, ROWS, HEADS * HD), BF16),
             v((SEQS, ROWS // 4, 4096), BF16),
@@ -636,7 +647,7 @@
             v((16, 32, 256), BF16),
             v((16, 32, 256), BF16),
             v((16, 32, 256), BF16),
-            dma((4,)),
+            dma((7,)),
             *[dma((2, 2, 20)) for _ in range(2)],
             *[dma((2, 2, 16)) for _ in range(2)],
             *[dma((2, 8)) for _ in range(2)],
@@ -647,10 +658,17 @@
             *[dma((15,)) for _ in range(2)],
         ],
         compiler_params=pltpu.CompilerParams(
-            collective_id=0, has_side_effects=True, vmem_limit_bytes=58 * 2**20
+            collective_id=0, has_side_effects=True, vmem_limit_bytes=44 * 2**20
         ),
         name="whole",
-    )(chosen, inverse, keys, values, gates, queries, cotangent, layer_input)
+    )(
+        chosen,
+        inverse,
+        *[
+            pltpu.with_memory_space_constraint(a, pltpu.HBM)
+            for a in (keys, values, gates, queries, cotangent, layer_input)
+        ],
+    )
 
 
 def on_device(queries, key_states, value_states, cotangent, gate_logits, layer_input, chosen):

time: 112 us -> 98.1 us (0.88)
  Pallas kernels: 103 us -> 92 us
  local copies, waits for them, and re-layouts: 6.93 us -> 4.03 us
    pallas_call x1, Pallas kernels: 103 us -> 92 us  [whole(): pl.pallas_call(whole_kernel, out_shape=[jax.ShapeDtypeStruct((SEQS, ROWS,...]
    unnamed x5 -> x7, local copies, waits for them, and re-layouts: 6.92 us -> 4.02 us
where the time goes in v1:
time: 98.1 us; the launch traced here: 96.9 us
  Pallas kernels  92 us (94%)
  local copies, waits for them, and re-layouts  4.03 us (4%)
    pallas_call x1, Pallas kernels, whole(): pl.pallas_call(whole_kernel, out_shape=[jax.ShapeDtypeStruct((SEQS, ROWS,...  92 us
    unnamed x7, local copies, waits for them, and re-layouts  4.02 us

profile of v1, /device:TPU:0, one launch (start us, length us, event | category | flops | bytes accessed | tf_op | source)
XLA Modules:
  0.0 96.9 jit_solution(6402129286279855353)
XLA Ops:
  0.6 0.1 iota_add_fusion
  0.7 0.7 copy.16
  1.4 0.2 select_reduce_fusion.inv_ref
  1.6 0.0 copy-start
  1.6 0.7 copy-done
  2.3 92.0 %whole.1 = (bf16[2,384,256]{2,1,0:T(8,128)(2,1)S(1)}, bf16[2,64,384]{2,1,0:T(8,128)(2,1)S(1)}, bf16[2,64,384]{2,1,0:T(8,128)(2,1)S(1)}, f32[32,256]{1,0:T(8,128)S(1)}) custom-call(s32[2,6,1,16]{3,2,1,0:T(1,128)S(1)} %copy-done, s32[2,6,192]{2,1,0:T(8,128)S(1)} %select_reduce_fusion.inv_ref, bf16[2,64,384]{2,1,0:T(8,128)(2,1)} %bitcast.10, ...), custom_call_target="tpu_custom_call" | custom-call | tf_op jit(solution)/shard_map/whole/pallas_call | solution.py:610
  94.3 0.7 copy.21
  95.0 0.6 copy.22
  95.7 0.6 copy.23
  96.3 0.6 copy.24
  (2 shorter events, 0.0 us)
Async XLA Ops:
  1.6 0.7 copy-start

commit v2 on v1

--- a/solution.py
+++ b/solution.py
@@ -296,10 +296,10 @@
 
 
 def whole_kernel(
-    ids_ref, inv_ref, k_hbm, v_hbm, gate_hbm, q_hbm, g_hbm, x_hbm,
+    ids_hbm, k_hbm, v_hbm, gate_hbm, q_hbm, g_hbm, x_hbm,
     dq_ref, kg_ref, vg_ref, wg_ref,
     kv0, kv1, table0, table1, mate0, mate1, acc0, acc1, sa0, ra0, sa1, ra1, sb0, rb0, sb1, rb1,
-    k_ref, v_ref, gate_ref, q_in, g_in, x_in, gates_t, rows_all, kvbuf, scores, packed, picks, final,
+    ids_ref, inv_ref, inv_v, k_ref, v_ref, gate_ref, q_in, g_in, x_in, gates_t, rows_all, kvbuf, scores, packed, picks, final,
     li_t, li_in, vsend, vland, rhs, w_out, w_own, w_mate, wsend, wland,
     l_sem, ag_s, ag_r, agp_s, agp_r, s_mate, r_mate, s_ring, r_ring, s_li, r_li, s_x, r_x, s_w, r_w, s_d, r_d,
 ):
@@ -316,7 +316,7 @@
     offsets = [(dz, dy) for dz in (2, 1, 3, 0) for dy in (2, 1, 3, 0)][:-1]
     kvs, tables = (kv0, kv1), (table0, table1)
 
-    pairs = ((k_hbm, k_ref), (v_hbm, v_ref), (x_hbm, x_in), (q_hbm, q_in), (g_hbm, g_in), (gate_hbm, gate_ref))
+    pairs = ((k_hbm, k_ref), (v_hbm, v_ref), (x_hbm, x_in), (q_hbm, q_in), (g_hbm, g_in), (gate_hbm, gate_ref), (ids_hbm, ids_ref))
     local = [pltpu.make_async_copy(a, b, l_sem.at[n]) for n, (a, b) in enumerate(pairs)]
     for d in local:
         d.start()
@@ -424,9 +424,9 @@
     def collect(s):
         def one(j, carry):
             for b in range(BPD):
-                total = picks[inv_ref[s, 0, j * BPD + b]]
+                total = picks[inv_ref[s * BPD, j * BPD + b]]
                 for q in range(1, BPD):
-                    total = total + picks[inv_ref[s, q, j * BPD + b]]
+                    total = total + picks[inv_ref[s * BPD + q, j * BPD + b]]
                 tables[s][j // 8, (j // 2) % 4, j % 2, b * BLK : (b + 1) * BLK] = total.astype(BF16)
             return carry
 
@@ -471,11 +471,20 @@
                 ).astype(BF16)
 
     steps[0][0]()
-    steps[1][0]()
+    local[6].wait()
+    spot = lax.broadcasted_iota(jnp.int32, (1, 256), 1)
+    for s in range(SEQS):
+        for qb in range(BPD):
+            slot = jnp.full((1, 256), BPD * TOPK, jnp.int32)
+            for k in range(TOPK):
+                slot = jnp.where(spot == ids_ref[s, qb, 0, k], qb * TOPK + k, slot)
+            inv_v[s * BPD + qb : s * BPD + qb + 1] = slot
+    to_scalar = pltpu.make_async_copy(inv_v, inv_ref, l_sem.at[8])
+    to_scalar.start()
     local[2].wait()
     lax.fori_loop(0, 4, turn_input, 0)
     steps[0][1]()
-    steps[1][1]()
+    steps[1][0]()
     lax.fori_loop(4, 8, turn_input, 0)
     for n in (1, 0, 2):
         li_copy(n).start()
@@ -483,11 +492,12 @@
         local[n].wait()
     for s in range(SEQS):
         gates_t[s] = jax.nn.sigmoid(gate_ref[s]).T
+    to_scalar.wait()
     picks[BPD * TOPK] = jnp.zeros((BLK, 2 * HD), F32)
     for n in range(2, 5):
         steps[0][n]()
-        if n < 4:
-            steps[1][n]()
+        if n != 3:
+            steps[1][n // 2]()
 
         def some(i, carry, n=n):
             at = (n - 2) * 4 + i
@@ -505,7 +515,7 @@
 
         return at
 
-    marks = [between(0, steps[1][4]), between(2, steps[1][5])]
+    marks = [between(0, steps[1][3]), between(2, steps[1][4]), between(4, steps[1][5])]
 
     def attend0(qb, carry):
         attend(0, qb)
@@ -517,7 +527,7 @@
     collect(0)
     reduces[0].share()
 
-    marks1 = [between(1, reduces[0].begin), between(3, reduces[0].middle), between(5, reduces[0].turn)]
+    marks1 = [between(2, reduces[0].begin), between(4, reduces[0].middle)]
 
     def attend1(qb, carry):
         attend(1, qb)
@@ -528,8 +538,9 @@
     lax.fori_loop(0, BPD, attend1, 0)
     collect(1)
     reduces[1].share()
+    reduces[0].turn()
+    reduces[1].begin()
     reduces[0].middle_b()
-    reduces[1].begin()
     reduces[1].middle()
     finish(0)
     reduces[1].turn()
@@ -539,7 +550,7 @@
     for n in range(3):
         frm = (tp + 3 - n) % 4
         rcopy(li_in.at[frm], li_in.at[frm], s_li.at[n], r_li.at[n], (kv, frm)).wait_recv()
-    mine_li = pltpu.make_async_copy(li_t.at[tp], li_in.at[tp], l_sem.at[6])
+    mine_li = pltpu.make_async_copy(li_t.at[tp], li_in.at[tp], l_sem.at[7])
     mine_li.start()
     mine_li.wait()
     landed(1)
@@ -552,30 +563,34 @@
             total = p if total is None else total + p
         return total.reshape(4, 32, 256)
 
-    def for_mate(i, carry):
-        w_out[pl.ds(i * 4, 4)] = product(other, i).astype(BF16)
-        return carry
-
-    def for_self(i, carry):
-        w_own[pl.ds(i * 4, 4)] = product(c, i)
-        return carry
-
-    lax.fori_loop(0, 4, for_mate, 0)
-    w_copy = rcopy(w_out, w_mate, s_w.at[0], r_w.at[0], partner)
-    w_copy.start()
-    lax.fori_loop(0, 4, for_self, 0)
-    w_copy.wait_recv()
-    w_own[...] = w_own[...] + w_mate[...].astype(F32)
-    wsend[...] = w_own[...].astype(BF16)
+    order = (2, 1, 3, 0)
     mine = kv // 2
+
+    def piece(dz):
+        return pl.ds(((z + dz) % 4) * 4, 4)
+
+    def w_copy(dz):
+        rows = piece(dz)
+        return rcopy(w_out.at[rows], w_mate.at[rows], s_w.at[dz], r_w.at[dz], partner)
 
     def d_copy(n):
         dz, dy = offsets[n]
         to = zy(z + dz, y + dy)
         return rcopy(wsend.at[to[0] // 2], wland.at[mine], s_d.at[n], r_d.at[n], to)
 
-    for n in range(len(offsets)):
-        d_copy(n).start()
+    for dz in order:
+        w_out[piece(dz)] = product(other, (z + dz) % 4).astype(BF16)
+        w_copy(dz).start()
+    for dz in order:
+        w_own[piece(dz)] = product(c, (z + dz) % 4)
+    for dz in order:
+        w_copy(dz).wait_recv()
+        value = w_own[piece(dz)] + w_mate[piece(dz)].astype(F32)
+        w_own[piece(dz)] = value
+        wsend[piece(dz)] = value.astype(BF16)
+        for n in range(len(offsets)):
+            if offsets[n][0] == dz:
+                d_copy(n).start()
     total = w_own[mine]
     for n, (dz, dy) in enumerate(offsets):
         frm = zy(z - dz, y - dy)
@@ -593,18 +608,18 @@
         li_copy(n).wait_send()
         for s in range(SEQS):
             x_copy(s, n).wait_send()
-    w_copy.wait_send()
+    for dz in order:
+        w_copy(dz).wait_send()
     for n in range(len(offsets)):
         d_copy(n).wait_send()
 
 
-def whole(chosen, inverse, keys, values, gates, queries, cotangent, layer_input):
+def whole(chosen, keys, values, gates, queries, cotangent, layer_input):
     v = pltpu.VMEM
     dma = pltpu.SemaphoreType.DMA
     wide = 2 * HD
     anywhere = pl.BlockSpec(memory_space=pltpu.HBM)
     onchip = pl.BlockSpec(memory_space=v)
-    smem = pl.BlockSpec(memory_space=pltpu.SMEM)
     keys_n = TOPK * BLK
     nrow = HEADS * BLK
     return pl.pallas_call(
@@ -615,7 +630,7 @@
             jax.ShapeDtypeStruct((SEQS, HD, ROWS), BF16),
             jax.ShapeDtypeStruct((32, 256), F32),
         ],
-        in_specs=[smem, smem] + [anywhere] * 6,
+        in_specs=[anywhere] * 7,
         out_specs=[onchip] * 4,
         scratch_shapes=[
             *[v((DEVS, ROWS, wide), BF16) for _ in range(2)],
@@ -624,6 +639,9 @@
             *[v((2, 4, HALF, wide), F32) for _ in range(2)],
             *[v((2, 6, 2, HALF, wide), BF16) for _ in range(4)],
             *[v((2, 6, QUART, wide), BF16) for _ in range(4)],
+            pltpu.SMEM((SEQS, BPD, 1, TOPK), jnp.int32),
+            pltpu.SMEM((SEQS * BPD, 256), jnp.int32),
+            v((SEQS * BPD, 256), jnp.int32),
             v((SEQS, HD, ROWS), BF16),
             v((SEQS, HD, ROWS), BF16),
             v((SEQS, HEADS, ROWS), F32),
@@ -647,14 +665,14 @@
             v((16, 32, 256), BF16),
             v((16, 32, 256), BF16),
             v((16, 32, 256), BF16),
-            dma((7,)),
+            dma((9,)),
             *[dma((2, 2, 20)) for _ in range(2)],
             *[dma((2, 2, 16)) for _ in range(2)],
             *[dma((2, 8)) for _ in range(2)],
             *[dma((2, 4, 6)) for _ in range(2)],
             *[dma((3,)) for _ in range(2)],
             *[dma((2, 3)) for _ in range(2)],
-            *[dma((1,)) for _ in range(2)],
+            *[dma((4,)) for _ in range(2)],
             *[dma((15,)) for _ in range(2)],
         ],
         compiler_params=pltpu.CompilerParams(
@@ -662,11 +680,9 @@
         ),
         name="whole",
     )(
-        chosen,
-        inverse,
         *[
             pltpu.with_memory_space_constraint(a, pltpu.HBM)
-            for a in (keys, values, gates, queries, cotangent, layer_input)
+            for a in (chosen, keys, values, gates, queries, cotangent, layer_input)
         ],
     )
 
@@ -675,13 +691,8 @@
     def turned(a):
         return jnp.swapaxes(a, 1, 2)
 
-    blocks = jnp.arange(DEVS * BPD, dtype=jnp.int32)
-    order = jnp.arange(TOPK, dtype=jnp.int32)[:, None]
-    first = jnp.arange(BPD, dtype=jnp.int32)[:, None, None] * TOPK
-    hit = chosen[:, :, 0, :, None] == blocks
-    inverse = jnp.min(jnp.where(hit, order + first, BPD * TOPK), axis=2)
     query_grad, key_grad, value_grad, weight_grad = whole(
-        chosen, inverse, turned(key_states), turned(value_states), turned(gate_logits),
+        chosen, turned(key_states), turned(value_states), turned(gate_logits),
         queries, cotangent, layer_input,
     )
     return query_grad, turned(key_grad), turned(value_grad), weight_grad

time: 98.1 us -> 90.7 us (0.925); the launches traced: 96.9 us -> 90.6 us
  Pallas kernels: 92 us -> 87.3 us
  local copies, waits for them, and re-layouts: 4.03 us -> 2.64 us
    pallas_call x1, Pallas kernels: 92 us -> 87.3 us  [whole(): pl.pallas_call(whole_kernel, out_shape=[jax.ShapeDtypeStruct((SEQS, ROWS,...]
    unnamed x7 -> x4, local copies, waits for them, and re-layouts: 4.02 us -> 2.64 us
where the time goes in v2:
time: 90.7 us; the launch traced here: 90.6 us
  Pallas kernels  87.3 us (96%)
  local copies, waits for them, and re-layouts  2.64 us (3%)
    pallas_call x1, Pallas kernels, whole(): pl.pallas_call(whole_kernel, out_shape=[jax.ShapeDtypeStruct((SEQS, ROWS,...  87.3 us
    unnamed x4, local copies, waits for them, and re-layouts  2.64 us

profile of v2, /device:TPU:0, one launch (start us, length us, event | category | flops | bytes accessed | tf_op | source)
XLA Modules:
  0.0 90.6 jit_solution(16149979839939036410)
XLA Ops:
  0.6 87.3 %whole.1 = (bf16[2,384,256]{2,1,0:T(8,128)(2,1)S(1)}, bf16[2,64,384]{2,1,0:T(8,128)(2,1)S(1)}, bf16[2,64,384]{2,1,0:T(8,128)(2,1)S(1)}, f32[32,256]{1,0:T(8,128)S(1)}) custom-call(s32[2,6,1,16]{3,2,1,0:T(1,128)} %ids_hbm.1, bf16[2,64,384]{2,1,0:T(8,128)(2,1)} %bitcast.7, bf16[2,64,384]{2,1,0:T(8,128)(2,1)} %bitcast.8, f32[2,4,384]{2,1,0:T(4,128)} %bitcast.9, ...), custom_call_target="tpu_custom_call" | custom-call | tf_op jit(solution)/shard_map/whole/pallas_call | solution.py:625
  88.0 0.7 copy.15
  88.7 0.6 copy.16
  89.4 0.6 copy.17
  90.0 0.6 copy.18

commit v3 on v2

--- a/solution.py
+++ b/solution.py
@@ -230,11 +230,6 @@
             dst = self.mate.at[(self.z + g) % 4, :, rows]
         return rcopy(src, dst, self.s_mate.at[h * 4 + g], self.r_mate.at[h * 4 + g], self.partner)
 
-    def share(self):
-        for g in (2, 1, 3, 0):
-            for h in range(2):
-                self.mate_copy(h, g).start()
-
     def part_a(self, h):
         rows = slice(h * HALF, (h + 1) * HALF)
 
@@ -299,7 +294,7 @@
     ids_hbm, k_hbm, v_hbm, gate_hbm, q_hbm, g_hbm, x_hbm,
     dq_ref, kg_ref, vg_ref, wg_ref,
     kv0, kv1, table0, table1, mate0, mate1, acc0, acc1, sa0, ra0, sa1, ra1, sb0, rb0, sb1, rb1,
-    ids_ref, inv_ref, inv_v, k_ref, v_ref, gate_ref, q_in, g_in, x_in, gates_t, rows_all, kvbuf, scores, packed, picks, final,
+    ids_ref, inv_ref, inv_v, k_ref, v_ref, gate_ref, q_in, g_in, x_in, gates_t, rows_all, kvbuf_a, kvbuf_b, scores_a, scores_b, packed_a, packed_b, picks, final,
     li_t, li_in, vsend, vland, rhs, w_out, w_own, w_mate, wsend, wland,
     l_sem, ag_s, ag_r, agp_s, agp_r, s_mate, r_mate, s_ring, r_ring, s_li, r_li, s_x, r_x, s_w, r_w, s_d, r_d,
 ):
@@ -315,6 +310,7 @@
     xs = [(kv, (tp + d) % 4) for d in (1, 2, 3)]
     offsets = [(dz, dy) for dz in (2, 1, 3, 0) for dy in (2, 1, 3, 0)][:-1]
     kvs, tables = (kv0, kv1), (table0, table1)
+    kvbufs, score_bufs, packs = (kvbuf_a, kvbuf_b), (scores_a, scores_b), (packed_a, packed_b)
 
     pairs = ((k_hbm, k_ref), (v_hbm, v_ref), (x_hbm, x_in), (q_hbm, q_in), (g_hbm, g_in), (gate_hbm, gate_ref), (ids_hbm, ids_ref))
     local = [pltpu.make_async_copy(a, b, l_sem.at[n]) for n, (a, b) in enumerate(pairs)]
@@ -373,16 +369,22 @@
             rows_all[at, h * BLK : (h + 1) * BLK] = jnp.where(low, qv, 0.0).astype(BF16)
             rows_all[at, nrow + h * BLK : nrow + (h + 1) * BLK] = jnp.where(low, 0.0, gv).astype(BF16)
 
-    def attend(s, qb):
+    def begin_block(s, qb, slot):
+        kvbuf, scores = kvbufs[slot], score_bufs[slot]
         at = s * BPD + qb
         kv_ref = kvs[s]
-        block = kv * BPD + qb
         picked = [ids_ref[s, qb, 0, k] for k in range(TOPK)]
         for k in range(TOPK):
             kvbuf[k * BLK : (k + 1) * BLK] = kv_ref[picked[k] // BPD, pl.ds((picked[k] % BPD) * BLK, BLK)]
         scores[...] = lax.dot_general(
             kvbuf[...], rows_all[at], (((1,), (1,)), ((), ())), preferred_element_type=F32
         )
+        return picked
+
+    def end_block(s, qb, slot, picked):
+        kvbuf, scores, packed = kvbufs[slot], score_bufs[slot], packs[slot]
+        at = s * BPD + qb
+        block = kv * BPD + qb
         qpos = block * BLK + lax.broadcasted_iota(jnp.int32, (BLK, nrow), 1) % BLK
         ahead = lax.broadcasted_iota(jnp.int32, (BLK, nrow), 0) - qpos
 
@@ -421,16 +423,33 @@
             [dq[h * BLK : (h + 1) * BLK] for h in range(HEADS)], axis=1
         ).astype(BF16)
 
+    def attend(s, pair):
+        blocks = (2 * pair, 2 * pair + 1)
+        ids = [begin_block(s, qb, slot) for slot, qb in enumerate(blocks)]
+        for slot, qb in enumerate(blocks):
+            end_block(s, qb, slot, ids[slot])
+
     def collect(s):
-        def one(j, carry):
-            for b in range(BPD):
-                total = picks[inv_ref[s * BPD, j * BPD + b]]
-                for q in range(1, BPD):
-                    total = total + picks[inv_ref[s * BPD + q, j * BPD + b]]
-                tables[s][j // 8, (j // 2) % 4, j % 2, b * BLK : (b + 1) * BLK] = total.astype(BF16)
-            return carry
-
-        lax.fori_loop(0, DEVS, one, 0)
+        table = tables[s]
+
+        def made(zz, yy, cc, b):
+            col = (zz * 8 + yy * 2 + cc) * BPD + b
+            total = picks[inv_ref[s * BPD, col]]
+            for q in range(1, BPD):
+                total = total + picks[inv_ref[s * BPD + q, col]]
+            table[zz, yy, cc, b * BLK : (b + 1) * BLK] = total.astype(BF16)
+
+        for g in (2, 1, 3, 0):
+
+            def one(i, carry, g=g):
+                for b in range(BPD // 2):
+                    made(i // 2, (y + g) % 4, i % 2, b)
+                    made((z + g) % 4, i // 2, i % 2, BPD // 2 + b)
+                return carry
+
+            lax.fori_loop(0, 8, one, 0)
+            for h in range(2):
+                reduces[s].mate_copy(h, g).start()
 
     quarter = ROWS // 4
 
@@ -515,7 +534,7 @@
 
         return at
 
-    marks = [between(0, steps[1][3]), between(2, steps[1][4]), between(4, steps[1][5])]
+    marks = [between(0, steps[1][3]), between(1, steps[1][4]), between(2, steps[1][5])]
 
     def attend0(qb, carry):
         attend(0, qb)
@@ -523,11 +542,10 @@
             mark(qb)
         return carry
 
-    lax.fori_loop(0, BPD, attend0, 0)
+    lax.fori_loop(0, BPD // 2, attend0, 0)
     collect(0)
-    reduces[0].share()
-
-    marks1 = [between(2, reduces[0].begin), between(4, reduces[0].middle)]
+
+    marks1 = [between(1, reduces[0].begin), between(2, reduces[0].middle)]
 
     def attend1(qb, carry):
         attend(1, qb)
@@ -535,17 +553,16 @@
             mark(qb)
         return carry
 
-    lax.fori_loop(0, BPD, attend1, 0)
+    lax.fori_loop(0, BPD // 2, attend1, 0)
     collect(1)
-    reduces[1].share()
+    reduces[1].begin()
     reduces[0].turn()
-    reduces[1].begin()
+    reduces[1].middle()
     reduces[0].middle_b()
-    reduces[1].middle()
+    reduces[1].turn()
     finish(0)
-    reduces[1].turn()
+    reduces[1].middle_b()
     landed(0)
-    reduces[1].middle_b()
     finish(1)
     for n in range(3):
         frm = (tp + 3 - n) % 4
@@ -650,9 +667,9 @@
             v((SEQS, ROWS // 4, 4096), BF16),
             v((SEQS, ROWS, HEADS), F32),
             v((SEQS * BPD, 2 * nrow, wide), BF16),
-            v((keys_n, wide), BF16),
-            v((keys_n, 2 * nrow), F32),
-            v((keys_n, 2 * nrow), BF16),
+            *[v((keys_n, wide), BF16) for _ in range(2)],
+            *[v((keys_n, 2 * nrow), F32) for _ in range(2)],
+            *[v((keys_n, 2 * nrow), BF16) for _ in range(2)],
             v((BPD * TOPK + 1, BLK, wide), F32),
             v((ROWS, wide), F32),
             v((4, 16, 2, 32, 192), BF16),
@@ -676,7 +693,7 @@
             *[dma((15,)) for _ in range(2)],
         ],
         compiler_params=pltpu.CompilerParams(
-            collective_id=0, has_side_effects=True, vmem_limit_bytes=44 * 2**20
+            collective_id=0, has_side_effects=True, vmem_limit_bytes=48 * 2**20
         ),
         name="whole",
     )(

time: 90.7 us -> 88 us (0.970)
  Pallas kernels: 87.3 us -> 84.6 us
    pallas_call x1, Pallas kernels: 87.3 us -> 84.6 us  [whole(): pl.pallas_call(whole_kernel, out_shape=[jax.ShapeDtypeStruct((SEQS, ROWS,...]
where the time goes in v3:
time: 88 us; the launch traced here: 87.9 us
  Pallas kernels  84.6 us (96%)
  local copies, waits for them, and re-layouts  2.64 us (3%)
    pallas_call x1, Pallas kernels, whole(): pl.pallas_call(whole_kernel, out_shape=[jax.ShapeDtypeStruct((SEQS, ROWS,...  84.6 us
    unnamed x4, local copies, waits for them, and re-layouts  2.64 us

profile of v3, /device:TPU:0, one launch (start us, length us, event | category | flops | bytes accessed | tf_op | source)
XLA Modules:
  0.0 87.9 jit_solution(3068744316157250659)
XLA Ops:
  0.6 84.6 %whole.1 = (bf16[2,384,256]{2,1,0:T(8,128)(2,1)S(1)}, bf16[2,64,384]{2,1,0:T(8,128)(2,1)S(1)}, bf16[2,64,384]{2,1,0:T(8,128)(2,1)S(1)}, f32[32,256]{1,0:T(8,128)S(1)}) custom-call(s32[2,6,1,16]{3,2,1,0:T(1,128)} %ids_hbm.1, bf16[2,64,384]{2,1,0:T(8,128)(2,1)} %bitcast.7, bf16[2,64,384]{2,1,0:T(8,128)(2,1)} %bitcast.8, f32[2,4,384]{2,1,0:T(4,128)} %bitcast.9, ...), custom_call_target="tpu_custom_call" | custom-call | tf_op jit(solution)/shard_map/whole/pallas_call | solution.py:642
  85.2 0.7 copy.15
  86.0 0.6 copy.16
  86.6 0.6 copy.17
  87.3 0.6 copy.18

commit v4 on v3

--- a/solution.py
+++ b/solution.py
@@ -294,7 +294,7 @@
     ids_hbm, k_hbm, v_hbm, gate_hbm, q_hbm, g_hbm, x_hbm,
     dq_ref, kg_ref, vg_ref, wg_ref,
     kv0, kv1, table0, table1, mate0, mate1, acc0, acc1, sa0, ra0, sa1, ra1, sb0, rb0, sb1, rb1,
-    ids_ref, inv_ref, inv_v, k_ref, v_ref, gate_ref, q_in, g_in, x_in, gates_t, rows_all, kvbuf_a, kvbuf_b, scores_a, scores_b, packed_a, packed_b, picks, final,
+    ids_ref, inv_ref, inv_v, k_ref, v_ref, gate_ref, q_in, g_in, x_in, gates_t, rows_all, kvbuf_a, kvbuf_b, kvbuf_c, scores_a, scores_b, scores_c, packed_a, packed_b, packed_c, picks, final,
     li_t, li_in, vsend, vland, rhs, w_out, w_own, w_mate, wsend, wland,
     l_sem, ag_s, ag_r, agp_s, agp_r, s_mate, r_mate, s_ring, r_ring, s_li, r_li, s_x, r_x, s_w, r_w, s_d, r_d,
 ):
@@ -310,7 +310,7 @@
     xs = [(kv, (tp + d) % 4) for d in (1, 2, 3)]
     offsets = [(dz, dy) for dz in (2, 1, 3, 0) for dy in (2, 1, 3, 0)][:-1]
     kvs, tables = (kv0, kv1), (table0, table1)
-    kvbufs, score_bufs, packs = (kvbuf_a, kvbuf_b), (scores_a, scores_b), (packed_a, packed_b)
+    kvbufs, score_bufs, packs = (kvbuf_a, kvbuf_b, kvbuf_c), (scores_a, scores_b, scores_c), (packed_a, packed_b, packed_c)
 
     pairs = ((k_hbm, k_ref), (v_hbm, v_ref), (x_hbm, x_in), (q_hbm, q_in), (g_hbm, g_in), (gate_hbm, gate_ref), (ids_hbm, ids_ref))
     local = [pltpu.make_async_copy(a, b, l_sem.at[n]) for n, (a, b) in enumerate(pairs)]
@@ -424,7 +424,7 @@
         ).astype(BF16)
 
     def attend(s, pair):
-        blocks = (2 * pair, 2 * pair + 1)
+        blocks = (3 * pair, 3 * pair + 1, 3 * pair + 2)
         ids = [begin_block(s, qb, slot) for slot, qb in enumerate(blocks)]
         for slot, qb in enumerate(blocks):
             end_block(s, qb, slot, ids[slot])
@@ -534,7 +534,7 @@
 
         return at
 
-    marks = [between(0, steps[1][3]), between(1, steps[1][4]), between(2, steps[1][5])]
+    marks = [between(0, steps[1][3]), between(1, steps[1][4])]
 
     def attend0(qb, carry):
         attend(0, qb)
@@ -542,10 +542,11 @@
             mark(qb)
         return carry
 
-    lax.fori_loop(0, BPD // 2, attend0, 0)
+    lax.fori_loop(0, BPD // 3, attend0, 0)
     collect(0)
-
-    marks1 = [between(1, reduces[0].begin), between(2, reduces[0].middle)]
+    steps[1][5]()
+
+    marks1 = [between(0, reduces[0].begin), between(1, reduces[0].middle)]
 
     def attend1(qb, carry):
         attend(1, qb)
@@ -553,7 +554,7 @@
             mark(qb)
         return carry
 
-    lax.fori_loop(0, BPD // 2, attend1, 0)
+    lax.fori_loop(0, BPD // 3, attend1, 0)
     collect(1)
     reduces[1].begin()
     reduces[0].turn()
@@ -667,9 +668,9 @@
             v((SEQS, ROWS // 4, 4096), BF16),
             v((SEQS, ROWS, HEADS), F32),
             v((SEQS * BPD, 2 * nrow, wide), BF16),
-            *[v((keys_n, wide), BF16) for _ in range(2)],
-            *[v((keys_n, 2 * nrow), F32) for _ in range(2)],
-            *[v((keys_n, 2 * nrow), BF16) for _ in range(2)],
+            *[v((keys_n, wide), BF16) for _ in range(3)],
+            *[v((keys_n, 2 * nrow), F32) for _ in range(3)],
+            *[v((keys_n, 2 * nrow), BF16) for _ in range(3)],
             v((BPD * TOPK + 1, BLK, wide), F32),
             v((ROWS, wide), F32),
             v((4, 16, 2, 32, 192), BF16),
@@ -693,7 +694,7 @@
             *[dma((15,)) for _ in range(2)],
         ],
         compiler_params=pltpu.CompilerParams(
-            collective_id=0, has_side_effects=True, vmem_limit_bytes=48 * 2**20
+            collective_id=0, has_side_effects=True, vmem_limit_bytes=52 * 2**20
         ),
         name="whole",
     )(

time: 88 us -> 84.9 us (0.965)
  Pallas kernels: 84.6 us -> 81.5 us
    pallas_call x1, Pallas kernels: 84.6 us -> 81.5 us  [whole(): pl.pallas_call(whole_kernel, out_shape=[jax.ShapeDtypeStruct((SEQS, ROWS,...]
where the time goes in v4:
time: 84.9 us; the launch traced here: 84.8 us
  Pallas kernels  81.5 us (96%)
  local copies, waits for them, and re-layouts  2.64 us (3%)
    pallas_call x1, Pallas kernels, whole(): pl.pallas_call(whole_kernel, out_shape=[jax.ShapeDtypeStruct((SEQS, ROWS,...  81.5 us
    unnamed x4, local copies, waits for them, and re-layouts  2.64 us

profile of v4, /device:TPU:0, one launch (start us, length us, event | category | flops | bytes accessed | tf_op | source)
XLA Modules:
  0.0 84.8 jit_solution(17070255713299965275)
XLA Ops:
  0.6 81.5 %whole.1 = (bf16[2,384,256]{2,1,0:T(8,128)(2,1)S(1)}, bf16[2,64,384]{2,1,0:T(8,128)(2,1)S(1)}, bf16[2,64,384]{2,1,0:T(8,128)(2,1)S(1)}, f32[32,256]{1,0:T(8,128)S(1)}) custom-call(s32[2,6,1,16]{3,2,1,0:T(1,128)} %ids_hbm.1, bf16[2,64,384]{2,1,0:T(8,128)(2,1)} %bitcast.7, bf16[2,64,384]{2,1,0:T(8,128)(2,1)} %bitcast.8, f32[2,4,384]{2,1,0:T(4,128)} %bitcast.9, ...), custom_call_target="tpu_custom_call" | custom-call | tf_op jit(solution)/shard_map/whole/pallas_call | solution.py:643
  82.1 0.7 copy.15
  82.9 0.6 copy.16
  83.5 0.6 copy.17
  84.1 0.6 copy.18

commit v5 on v4

--- a/solution.py
+++ b/solution.py
@@ -544,9 +544,10 @@
 
     lax.fori_loop(0, BPD // 3, attend0, 0)
     collect(0)
+    reduces[0].begin()
     steps[1][5]()
 
-    marks1 = [between(0, reduces[0].begin), between(1, reduces[0].middle)]
+    marks1 = [between(0, reduces[0].middle), between(1, reduces[0].turn)]
 
     def attend1(qb, carry):
         attend(1, qb)
@@ -557,7 +558,6 @@
     lax.fori_loop(0, BPD // 3, attend1, 0)
     collect(1)
     reduces[1].begin()
-    reduces[0].turn()
     reduces[1].middle()
     reduces[0].middle_b()
     reduces[1].turn()

time: 84.9 us -> 84.9 us (level)
  no operation moved by 1% of the time
where the time goes in v5:
time: 84.9 us; the launch traced here: 84.8 us
  Pallas kernels  81.5 us (96%)
  local copies, waits for them, and re-layouts  2.64 us (3%)
    pallas_call x1, Pallas kernels, whole(): pl.pallas_call(whole_kernel, out_shape=[jax.ShapeDtypeStruct((SEQS, ROWS,...  81.5 us
    unnamed x4, local copies, waits for them, and re-layouts  2.64 us

profile of v5, /device:TPU:0, one launch (start us, length us, event | category | flops | bytes accessed | tf_op | source)
XLA Modules:
  0.0 84.8 jit_solution(14727056840482763268)
XLA Ops:
  0.6 81.5 %whole.1 = (bf16[2,384,256]{2,1,0:T(8,128)(2,1)S(1)}, bf16[2,64,384]{2,1,0:T(8,128)(2,1)S(1)}, bf16[2,64,384]{2,1,0:T(8,128)(2,1)S(1)}, f32[32,256]{1,0:T(8,128)S(1)}) custom-call(s32[2,6,1,16]{3,2,1,0:T(1,128)} %ids_hbm.1, bf16[2,64,384]{2,1,0:T(8,128)(2,1)} %bitcast.7, bf16[2,64,384]{2,1,0:T(8,128)(2,1)} %bitcast.8, f32[2,4,384]{2,1,0:T(4,128)} %bitcast.9, ...), custom_call_target="tpu_custom_call" | custom-call | tf_op jit(solution)/shard_map/whole/pallas_call | solution.py:643
  82.1 0.7 copy.15
  82.9 0.6 copy.16
  83.5 0.6 copy.17
  84.2 0.6 copy.18
